TPU v7x, 256 devices: a whole 4x4x8 slice. The times are simulated.
256 devices in a mesh: sp: 64 (over z, x, core), tp: 4 (over y).
Axes of the slice: x: 4, y: 4, z: 8, core: 2. Of those that a mesh axis runs over, the one named last changes fastest.
Arguments:
- stream: bfloat16 [8192, 2048], P(('sp', 'tp')), may hold values from -2.5 to 2.5
- recurrence_input: bfloat16 [8192, 2, 1024], P('sp', None, 'tp'), may hold values from -6 to 6
- output_gate_input: bfloat16 [8192, 2, 1024], P('sp', None, 'tp'), may hold values from -6 to 6
- convolution_taps: bfloat16 [4, 2, 1024], P(None, None, 'tp'), may hold values from -4 to 4
- first_group_gates: bfloat16 [2, 16, 64, 64], P(None, 'tp'), may hold values from -0.75 to 0.75
- second_group_gates: bfloat16 [2, 8, 128, 128], P(None, 'tp'), may hold values from -0.5 to 0.5
- channel_decay: float32 [2, 1024], P(None, 'tp'), may hold values from 4.7 to 13.6
- position_log_extra: float32 [8192, 2, 1024], P('sp', None, 'tp'), may hold values from -1.4 to 0, as said below
- recurrence_output_weight: bfloat16 [2, 1024, 2048], P(None, 'tp'), may hold values from -0.125 to 0.125
- first_norm_gain: float32 [2048], replicated, may hold values from 0.1 to 1.9
- first_norm_bias: float32 [2048], replicated, may hold values from -1.75 to 1.75
- routed_expert_index: int32 [8192, 4], P('sp'), may hold values from 0 to 63, all different within a row; in each aligned block of 32 rows (0 to 31, 32 to 63, ...) at most 2 rows name the same one
- routed_expert_weight: float32 [8192, 4], P('sp'), may hold values from 0.25 to 1
- routed_gate_weight: bfloat16 [64, 2048, 512], P('sp', None, 'tp'), may hold values from -0.125 to 0.125
- routed_up_weight: bfloat16 [64, 2048, 512], P('sp', None, 'tp'), may hold values from -0.125 to 0.125
- routed_down_weight: bfloat16 [64, 512, 2048], P('sp', 'tp'), may hold values from -0.25 to 0.25
- shared_gate_weight: bfloat16 [2048, 512], replicated, may hold values from -0.125 to 0.125
- shared_up_weight: bfloat16 [2048, 512], replicated, may hold values from -0.125 to 0.125
- shared_down_weight: bfloat16 [512, 2048], replicated, may hold values from -0.25 to 0.25
- second_norm_gain: float32 [2048], replicated, may hold values from 0.1 to 1.9
- second_norm_bias: float32 [2048], replicated, may hold values from -1.75 to 1.75
Outputs:
- result: bfloat16 [8192, 2048], P(('sp', 'tp'))
Inputs may be any that keep to these rules, and one draw needn't show every extreme that they name: `routed_expert_index`: each row names 4 different experts. In each aligned block of 32 rows no expert is named more than 2 times, and in some block an expert is named exactly 2 times. `position_log_extra`: every entry is negative.
All inputs are finite; a program needn't handle non-finite values.
Results may differ from a plain program's by a relative error of at most 0.015.
Values may be sent and summed in bfloat16 or wider, within the bound.
A program may use at most 64 MiB of HBM per device.

v0:
```python
import jax
import jax.numpy as jnp
from jax import lax
from jax.sharding import PartitionSpec as P

RESIDUAL_SCALE = 8.0**0.25
NORM_EPSILON = 1e-05


def copy_for_each(shard, axis):
    count = lax.axis_size(axis)
    return lax.all_to_all(
        jnp.broadcast_to(shard[None], (count, *shard.shape)), axis, 0, 0, tiled=True
    )


def all_in_one(shard, axis):
    leaves = jax.tree.leaves(shard)
    sequence = sorted(range(len(leaves)), key=lambda k: -leaves[k].size)
    width = (1, *leaves[sequence[0]].shape)[-1]
    lines = [
        jnp.pad(leaves[k].reshape(-1), (0, -leaves[k].size % width)).reshape(-1, width)
        for k in sequence
    ]
    both, at, found = (copy_for_each(jnp.concatenate(lines), axis), 0, {})
    for k, line in zip(sequence, lines):
        slab = both[:, at : at + len(line)].reshape(len(both), -1)
        found[k] = slab[:, : leaves[k].size].reshape(-1, *leaves[k].shape)
        at += len(line)
    numbers = iter(range(len(leaves)))
    return jax.tree.map(lambda _: found[next(numbers)], shard)


def joined_by_halves(pieces, combine):
    while len(jax.tree.leaves(pieces)[0]) > 1:
        pieces = jax.vmap(combine)(
            *(jax.tree.map(lambda part: part[side::2], pieces) for side in (0, 1))
        )
    return jax.tree.map(lambda part: part[0], pieces)


def entering(shard, axis, combine, identity):
    count, mine = (lax.axis_size(axis), lax.axis_index(axis))
    passed = jnp.arange(count) < mine

    def kept(part, zero, own):
        part = jnp.where(
            passed.reshape(-1, *(1 for _ in own.shape)), part, jnp.asarray(zero, own.dtype)
        )
        return part

    pieces = all_in_one(shard, axis)
    return joined_by_halves(jax.tree.map(kept, pieces, identity, shard), combine)


def shifted(shard, axis, by):
    count = lax.axis_size(axis)
    pairs = [(i, i + by) for i in range(count) if 0 <= i + by < count]
    return lax.ppermute(shard, axis, pairs)


def cut_along(shard, dim, count):
    dims = shard.shape
    pieces = shard.reshape(*dims[:dim], count, dims[dim] // count, *dims[dim + 1 :])
    return jnp.moveaxis(pieces, dim, 0)


def summed_on_arrival(shard, axis, dim):
    count = lax.axis_size(axis)
    pieces = lax.all_to_all(cut_along(shard, dim, count), axis, 0, 0, tiled=True)
    return jnp.sum(pieces.astype(jnp.float32), axis=0)


def layer_norm(values, gain_vec, bias_vec):
    row_mean = jnp.mean(values, axis=-1, keepdims=True)
    spread = jnp.mean(jnp.square(values - row_mean), axis=-1, keepdims=True)
    return (values - row_mean) * lax.rsqrt(spread + NORM_EPSILON) * gain_vec + bias_vec


def block_gates(conv_rows, weights, head_size):
    length = conv_rows.shape[0]
    head_rows = conv_rows.reshape(length, -1, head_size)
    pre_act = jnp.einsum("thc,ghcd->gthd", head_rows, weights, preferred_element_type=jnp.float32)
    gate_pair = jax.nn.sigmoid(pre_act).reshape(2, length, -1)
    return (gate_pair[0], gate_pair[1])


def chain_link(first_part, second_part):
    return (first_part[0] * second_part[0], second_part[0] * first_part[1] + second_part[1])


def carried(totals):
    unity = jnp.ones_like(totals[0])
    nought = jnp.zeros_like(totals[1])
    return entering(totals, "sp", chain_link, (unity, nought))[1]


def expert_terms(picked, letters, gate_w, up_w, down_w):
    gate_form = letters + "d,ldf->" + letters + "f"
    down_form = letters + "f,lfd->" + letters + "d"
    gated = jnp.einsum(gate_form, picked, gate_w, preferred_element_type=jnp.float32)
    lifted = jnp.einsum(gate_form, picked, up_w, preferred_element_type=jnp.float32)
    hidden = (jax.nn.silu(gated) * lifted).astype(jnp.bfloat16)
    return jnp.einsum(down_form, hidden, down_w, preferred_element_type=jnp.float32)


def shards(
    stream,
    recurrence_input,
    output_gate_input,
    convolution_taps,
    first_group_gates,
    second_group_gates,
    channel_decay,
    position_log_extra,
    recurrence_output_weight,
    first_norm_gain,
    first_norm_bias,
    routed_expert_index,
    routed_expert_weight,
    routed_gate_weight,
    routed_up_weight,
    routed_down_weight,
    shared_gate_weight,
    shared_up_weight,
    shared_down_weight,
    second_norm_gain,
    second_norm_bias,
):
    length = recurrence_input.shape[0]
    tap_count = convolution_taps.shape[0]
    border = shifted(recurrence_input[length - (tap_count - 1) :], "sp", 1)
    padded = jnp.concatenate([border, recurrence_input], axis=0).astype(jnp.float32)
    tap_weights = convolution_taps.astype(jnp.float32)
    summed = tap_weights[0] * padded[0:length]
    for offset in range(1, tap_count):
        summed = summed + tap_weights[offset] * padded[offset : offset + length]
    conv_rows = summed.astype(jnp.bfloat16)
    recur_a, input_a = block_gates(conv_rows[:, 0], first_group_gates, first_group_gates.shape[-1])
    recur_b, input_b = block_gates(
        conv_rows[:, 1], second_group_gates, second_group_gates.shape[-1]
    )
    recurrence_gate = jnp.stack([recur_a, recur_b], axis=1)
    input_gate = jnp.stack([input_a, input_b], axis=1)
    decay_logarithm = -8.0 * recurrence_gate * jax.nn.softplus(-channel_decay) + position_log_extra
    decay_rate = jnp.exp(decay_logarithm)
    driving = (
        jnp.sqrt(-jnp.expm1(2.0 * decay_logarithm)) * input_gate * conv_rows.astype(jnp.float32)
    )
    running = jnp.cumsum(decay_logarithm, axis=0)
    tail_sum = jnp.sum(jnp.exp(running[-1] - running) * driving, axis=0)
    incoming = carried((jnp.exp(running[-1]), tail_sum))
    opening = driving[:1] + decay_rate[:1] * incoming
    started = jnp.concatenate([opening, driving[1:]], axis=0)
    states = lax.associative_scan(chain_link, (decay_rate, started), axis=0)[1]
    branch_output = (jax.nn.gelu(output_gate_input.astype(jnp.float32)) * states).astype(
        jnp.bfloat16
    )
    tp_count = lax.axis_size("tp")
    quarter = length // tp_count
    mixed = summed_on_arrival(
        jnp.einsum(
            "tgc,gcd->td",
            branch_output,
            recurrence_output_weight,
            preferred_element_type=jnp.float32,
        ).astype(jnp.bfloat16),
        "tp",
        0,
    )
    normed = layer_norm(
        RESIDUAL_SCALE * stream.astype(jnp.float32) + mixed, first_norm_gain, first_norm_bias
    ).astype(jnp.bfloat16)
    width = normed.shape[1]
    top_count = routed_expert_index.shape[1]
    local_count = routed_gate_weight.shape[0]
    expert_count = local_count * lax.axis_size("sp")
    capacity = max(2, 5 * quarter * top_count // (4 * expert_count))
    block_ids = routed_expert_index.reshape(tp_count, quarter * top_count)
    onehot = (
        block_ids[:, :, None] == jnp.arange(expert_count, dtype=jnp.int32)[None, None, :]
    ).astype(jnp.int32)
    slot_ranks = jnp.sum((jnp.cumsum(onehot, axis=1) - onehot) * onehot, axis=2)
    own_index = lax.axis_index("tp")
    own_ids = lax.dynamic_index_in_dim(block_ids, own_index, 0, keepdims=False)
    own_ranks = lax.dynamic_index_in_dim(slot_ranks, own_index, 0, keepdims=False)
    blank_row = jnp.zeros((1, width), jnp.bfloat16)
    padded_rows = jnp.concatenate([normed, blank_row], axis=0)
    targets = own_ids * capacity + own_ranks
    sources = jnp.arange(quarter * top_count, dtype=jnp.int32) // top_count
    table = jnp.full((expert_count * capacity,), quarter, jnp.int32).at[targets].set(sources)
    outgoing = jnp.take(padded_rows, table, axis=0).reshape(expert_count, capacity, width)
    arrived = lax.all_to_all(outgoing, "sp", split_axis=0, concat_axis=0, tiled=True)
    slots = arrived.shape[1]
    fanned = lax.all_gather(arrived[None], "tp", axis=0, tiled=True)
    shaped = fanned.reshape(tp_count, -1, local_count, slots, width)
    partial_value = expert_terms(
        shaped, "xslc", routed_gate_weight, routed_up_weight, routed_down_weight
    )
    summed_rows = summed_on_arrival(partial_value.astype(jnp.bfloat16), "tp", 0)
    leaving = summed_rows.astype(jnp.bfloat16).reshape(-1, slots, width)
    returned = lax.all_to_all(leaving, "sp", split_axis=0, concat_axis=0, tiled=True)
    picked_rows = returned.reshape(expert_count * capacity, width)[own_ids * capacity + own_ranks]
    own_weights = lax.dynamic_slice_in_dim(routed_expert_weight, own_index * quarter, quarter, 0)
    routed = jnp.sum(
        own_weights[:, :, None]
        * picked_rows.reshape(quarter, top_count, width).astype(jnp.float32),
        axis=1,
    )
    shared_hidden = (
        jax.nn.silu(jnp.dot(normed, shared_gate_weight, preferred_element_type=jnp.float32))
        * jnp.dot(normed, shared_up_weight, preferred_element_type=jnp.float32)
    ).astype(jnp.bfloat16)
    shared_out = jnp.dot(shared_hidden, shared_down_weight, preferred_element_type=jnp.float32)
    final = layer_norm(
        RESIDUAL_SCALE * normed.astype(jnp.float32) + (shared_out + routed),
        second_norm_gain,
        second_norm_bias,
    )
    return final.astype(jnp.bfloat16)


def solution(mesh):
    in_specs = (
        P(("sp", "tp"), None),
        P("sp", None, "tp"),
        P("sp", None, "tp"),
        P(None, None, "tp"),
        P(None, "tp", None, None),
        P(None, "tp", None, None),
        P(None, "tp"),
        P("sp", None, "tp"),
        P(None, "tp", None),
        P(),
        P(),
        P("sp", None),
        P("sp", None),
        P("sp", None, "tp"),
        P("sp", None, "tp"),
        P("sp", "tp", None),
        P(),
        P(),
        P(),
        P(),
        P(),
    )
    out_specs = P(("sp", "tp"), None)
    return jax.shard_map(shards, mesh=mesh, in_specs=in_specs, out_specs=out_specs, check_vma=False)
```

profile of v0, /device:TPU:1, one launch (start us, length us, event | category | flops | bytes accessed | tf_op | source)
XLA Modules:
  0.0 205.7 jit_solution(793034132163294517)
XLA Ops:
  6.5 1.1 copy.130
  7.6 4.5 %collective-permute-start = (bf16[3,2,256]{2,0,1:T(4,128)(2,1)S(1)}, bf16[3,2,256]{2,0,1:T(4,128)(2,1)S(1)}, u32[]{:S(2)}, u32[]{:S(2)}) collective-permute-start(bf16[3,2,256]{2,0,1:T(4,128)(2,1)S(1)} %slice.395), channel_id=1, source_target_pairs={{0,4},{4,8},{8,12},{12,16},{16,20},{20,24},{24,28},{28,32},{32,36}... | collective-permute-start | bytes 9224 | tf_op jit(solution)/shard_map/ppermute | solution.py:59
  12.1 0.7 convert_element_type.67
  12.9 0.7 fusion.84
  13.6 0.8 copy.147
  14.4 0.7 reshape.136
  15.4 0.3 fusion.20
  16.0 0.3 fusion.16
  16.4 1.0 fusion.101
  17.6 0.6 slice_bitcast_fusion
  18.1 0.6 fusion.99
  18.8 0.8 copy.166
  19.6 1.2 fusion.52
  20.9 0.7 broadcast_in_dim.61
  21.6 11.3 %all-to-all-start = ((f32[64,4,256]{2,1,0:T(4,128)}), f32[64,4,256]{2,1,0:T(4,128)S(1)}, u32[]{:S(2)}, u32[]{:S(2)}) async-start(f32[64,4,256]{2,1,0:T(4,128)} %broadcast_in_dim.61), calls=%async_computation | async-start | bytes 524288 | tf_op jit(solution)/shard_map/all_to_all | solution.py:12
  32.9 0.8 fusion.60
  34.0 0.9 select_reduce_fusion
  34.9 0.7 fusion.90
  35.6 1.5 scatter_custom_fusion
  37.1 0.7 slice.345
  37.9 0.7 slice.343
  38.7 7.3 %all-to-all-done = f32[64,4,256]{2,1,0:T(4,128)S(1)} async-done(((f32[64,4,256]{2,1,0:T(4,128)}), f32[64,4,256]{2,1,0:T(4,128)S(1)}, u32[]{:S(2)}, u32[]{:S(2)}) %all-to-all-start) | async-done | bytes 262176 | tf_op jit(solution)/shard_map/all_to_all | solution.py:12
  46.2 0.6 slice.315
  46.8 0.6 slice.316
  47.5 0.9 fusion.109
  49.0 1.0 fusion.106
  51.7 1.3 fusion.1
  53.0 4.3 %all-to-all-start.1 = ((bf16[4,32,2048]{2,1,0:T(8,128)(2,1)}), bf16[4,32,2048]{2,1,0:T(8,128)(2,1)S(1)}, u32[]{:S(2)}, u32[]{:S(2)}) async-start(bf16[4,32,2048]{2,1,0:T(8,128)(2,1)} %bitcast.17), calls=%async_computation.1 | async-start | bytes 1048576 | tf_op jit(solution)/shard_map/all_to_all | solution.py:70
  57.5 8.8 %all-to-all-done.1 = bf16[4,32,2048]{2,1,0:T(8,128)(2,1)S(1)} async-done(((bf16[4,32,2048]{2,1,0:T(8,128)(2,1)}), bf16[4,32,2048]{2,1,0:T(8,128)(2,1)S(1)}, u32[]{:S(2)}, u32[]{:S(2)}) %all-to-all-start.1) | async-done | bytes 524320 | tf_op jit(solution)/shard_map/all_to_all | solution.py:70
  67.0 0.9 gather_fusion
  67.9 1.1 gather.10
  69.0 1.6 broadcast_select_fusion
  70.6 23.1 %all_to_all.25 = bf16[64,2,2048]{2,1,0:T(2,128)(2,1)S(1)} all-to-all(bf16[64,2,2048]{2,1,0:T(2,128)(2,1)S(1)} %broadcast_select_fusion), channel_id=1, replica_groups=mesh['sp'=64,'tp'=4] {'sp'}, dimensions={0} | all-to-all | bytes 1048576 | tf_op jit(solution)/shard_map/all_to_all | solution.py:193
  93.8 1.0 copy.148
  94.8 27.8 %all-gather.3.cloned.1.call-done = bf16[256,2,2048]{2,0,1:T(8,128)(2,1)} async-done(((bf16[64,2,2048]{2,0,1:T(8,128)(2,1)}), bf16[256,2,2048]{2,0,1:T(8,128)(2,1)}) %all-gather.3.cloned.1.call-update) | async-done | bytes 2097168 | tf_op jit(solution)/shard_map/all_gather | solution.py:195
  122.6 2.4 %fusion.7 = f32[4,64,1,2,128]{4,1,3,0,2:T(8,128)S(1)} fusion(bf16[4,64,2,2048]{3,1,0,2:T(8,128)(2,1)} %bitcast.118, bf16[1,2048,128]{2,1,0:T(8,128)(2,1)} %param.34), kind=kOutput, calls=%fused_computation.14 | convolution fusion | flops 268435456 | bytes 2883584 | tf_op jit(solution)/shard_map/xslcd,ldf->xslcf/dot_general | solution.py:101
  125.0 5.2 %fusion = bf16[4,1,64,1,2,2048]{5,2,4,3,1,0:T(8,128)(2,1)} fusion(bf16[4,64,2,2048]{3,1,0,2:T(8,128)(2,1)} %bitcast.119, bf16[1,128,2048]{2,1,0:T(8,128)(2,1)S(1)} %copy-done.2, bf16[1,2048,128]{2,1,0:T(8,128)(2,1)S(1)} %copy-done.3, f32[4,64,1,2,128]{4,1,3,0,2:T(8,128)S(1)} %fusion.7), kind=kOutput, calls=%fused_computation.4 | convolution fusion | flops 538312704 | bytes 5505024 | tf_op jit(solution)/shard_map/xslcf,lfd->xslcd/dot_general | solution.py:104
  130.2 28.9 %all_to_all.26 = bf16[4,1,64,1,2,2048]{5,2,4,3,1,0:T(8,128)(2,1)S(1)} all-to-all(bf16[4,1,64,1,2,2048]{5,2,4,3,1,0:T(8,128)(2,1)} %fusion), channel_id=1, replica_groups=mesh['sp'=64,'tp'=4] {'tp'}, dimensions={0} | all-to-all | bytes 4194304 | tf_op jit(solution)/shard_map/all_to_all | solution.py:70
  159.2 0.4 bitcast_reduce_fusion
  159.5 1.3 copy.153
  160.9 11.9 %all-to-all-start.4 = ((bf16[64,2,2048]{2,1,0:T(2,128)(2,1)}), bf16[64,2,2048]{2,1,0:T(2,128)(2,1)S(1)}, u32[]{:S(2)}, u32[]{:S(2)}) async-start(bf16[64,2,2048]{2,1,0:T(2,128)(2,1)} %copy.153), calls=%async_computation.4 | async-start | bytes 1048576 | tf_op jit(solution)/shard_map/all_to_all | solution.py:202
  173.0 2.7 %fusion.118 = f32[32,512]{1,0:T(8,128)} fusion(bf16[32,2048]{1,0:T(8,128)(2,1)S(1)} %add_convert_fusion.1, bf16[2048,512]{1,0:T(8,128)(2,1)} %param.37), kind=kOutput, calls=%fused_computation.192 | convolution fusion | flops 67108864 | bytes 2293760 | tf_op jit(solution)/shard_map/dot_general | solution.py:211
  175.6 14.8 %all-to-all-done.4 = bf16[64,2,2048]{2,1,0:T(2,128)(2,1)S(1)} async-done(((bf16[64,2,2048]{2,1,0:T(2,128)(2,1)}), bf16[64,2,2048]{2,1,0:T(2,128)(2,1)S(1)}, u32[]{:S(2)}, u32[]{:S(2)}) %all-to-all-start.4) | async-done | bytes 524320 | tf_op jit(solution)/shard_map/all_to_all | solution.py:202
  190.7 1.7 gather_fusion.1
  192.4 1.4 reshape.143
  193.8 0.7 multiply_reduce_fusion
  194.5 3.3 %fusion.117 = (f32[32]{0:T(128)S(1)}, f32[32,2048]{1,0:T(8,128)S(1)}) fusion(f32[32,2048]{1,0:T(8,128)S(1)} %multiply_reduce_fusion, bf16[512,2048]{1,0:T(8,128)(2,1)} %param.39, bf16[32,2048]{1,0:T(8,128)(2,1)S(1)} %add_convert_fusion.1, bf16[2048,512]{1,0:T(8,128)(2,1)} %param.38, f32[32,512]{1,0:T(8,128)} %fusion.118), kind=kOutput, calls=%fused_computation.191 | convolution fusion | flops 134643680 | bytes 4915328 | tf_op jit(solution)/shard_map/dot_general | solution.py:214
  198.0 0.8 add_convert_fusion
  (181 shorter events, 4.9 us)
Async XLA Ops:
  6.5 45.1 %copy-start = (bf16[2,256,2048]{2,1,0:T(8,128)(2,1)S(1)}, bf16[2,256,2048]{2,1,0:T(8,128)(2,1)}, u32[]{:S(2)}) copy-start(bf16[2,256,2048]{2,1,0:T(8,128)(2,1)} %param.29) | copy-start | bytes 6291460
  6.5 8.9 %copy-start.19 = (bf16[2,4,64,64]{3,2,1,0:T(8,128)(2,1)S(1)}, bf16[2,4,64,64]{3,2,1,0:T(8,128)(2,1)}, u32[]{:S(2)}) copy-start(bf16[2,4,64,64]{3,2,1,0:T(8,128)(2,1)} %param.25) | copy-start | bytes 196612
  7.6 7.4 %collective-permute-start = (bf16[3,2,256]{2,0,1:T(4,128)(2,1)S(1)}, bf16[3,2,256]{2,0,1:T(4,128)(2,1)S(1)}, u32[]{:S(2)}, u32[]{:S(2)}) collective-permute-start(bf16[3,2,256]{2,0,1:T(4,128)(2,1)S(1)} %slice.395), channel_id=1, source_target_pairs={{0,4},{4,8},{8,12},{12,16},{16,20},{20,24},{24,28},{28,32},{32,36}... | collective-permute-start | bytes 9224 | tf_op jit(solution)/shard_map/ppermute | solution.py:59
  12.8 2.5 %copy-start.7 = (f32[2,256]{1,0:T(2,128)}, f32[2,256]{1,0:T(2,128)S(1)}, u32[]{:S(2)}) copy-start(f32[2,256]{1,0:T(2,128)S(1)} %get-tuple-element.37) | copy-start | bytes 6148
  12.8 2.5 %copy-start.8 = (f32[2,256]{1,0:T(2,128)}, f32[2,256]{1,0:T(2,128)S(1)}, u32[]{:S(2)}) copy-start(f32[2,256]{1,0:T(2,128)S(1)} %get-tuple-element.38) | copy-start | bytes 6148
  12.8 2.5 %copy-start.9 = (f32[2,256]{1,0:T(2,128)}, f32[2,256]{1,0:T(2,128)S(1)}, u32[]{:S(2)}) copy-start(f32[2,256]{1,0:T(2,128)S(1)} %get-tuple-element.39) | copy-start | bytes 6148
  12.9 2.5 %copy-start.10 = (f32[2,256]{1,0:T(2,128)}, f32[2,256]{1,0:T(2,128)S(1)}, u32[]{:S(2)}) copy-start(f32[2,256]{1,0:T(2,128)S(1)} %get-tuple-element.40) | copy-start | bytes 6148
  15.0 0.9 copy-start.20
  19.6 1.2 copy-start.15
  21.6 24.4 %all-to-all-start = ((f32[64,4,256]{2,1,0:T(4,128)}), f32[64,4,256]{2,1,0:T(4,128)S(1)}, u32[]{:S(2)}, u32[]{:S(2)}) async-start(f32[64,4,256]{2,1,0:T(4,128)} %broadcast_in_dim.61), calls=%async_computation | async-start | bytes 524288 | tf_op jit(solution)/shard_map/all_to_all | solution.py:12
  35.6 12.9 %copy-start.17 = (s32[128]{0:T(128)}, s32[128]{0:T(128)S(1)}, u32[]{:S(2)}) copy-start(s32[128]{0:T(128)S(1)} %fusion.90) | copy-start | bytes 1540
  48.9 1.2 copy-start.5
  50.3 1.2 copy-start.6
  50.8 0.9 copy-start.4
  51.7 5.6 %copy-start.21 = (s32[128]{0:T(128)S(1)}, s32[128]{0:T(128)}, u32[]{:S(2)}) copy-start(s32[128]{0:T(128)} %scatter_custom_fusion) | copy-start | bytes 1540
  51.7 14.7 %copy-start.1 = (bf16[32,2048]{1,0:T(8,128)(2,1)S(1)}, bf16[32,2048]{1,0:T(8,128)(2,1)}, u32[]{:S(2)}) copy-start(bf16[32,2048]{1,0:T(8,128)(2,1)} %param.21) | copy-start | bytes 393220
  53.0 13.8 %copy-start.11 = (f32[2048]{0:T(1024)S(1)}, f32[2048]{0:T(1024)}, u32[]{:S(2)}) copy-start(f32[2048]{0:T(1024)} %param.31) | copy-start | bytes 24580
  53.0 13.8 %copy-start.12 = (f32[2048]{0:T(1024)S(1)}, f32[2048]{0:T(1024)}, u32[]{:S(2)}) copy-start(f32[2048]{0:T(1024)} %param.30) | copy-start | bytes 24580
  53.0 13.3 %all-to-all-start.1 = ((bf16[4,32,2048]{2,1,0:T(8,128)(2,1)}), bf16[4,32,2048]{2,1,0:T(8,128)(2,1)S(1)}, u32[]{:S(2)}, u32[]{:S(2)}) async-start(bf16[4,32,2048]{2,1,0:T(8,128)(2,1)} %bitcast.17), calls=%async_computation.1 | async-start | bytes 1048576 | tf_op jit(solution)/shard_map/all_to_all | solution.py:70
  57.3 65.3 %all-gather.3.cloned.1.call-start = ((), (), s32[]{:S(2)}) async-start(), calls=%async_computation.5 | async-start | bytes 2621440 | tf_op jit(solution)/shard_map/all_gather | solution.py:195
  94.7 30.2 %copy-start.2 = (bf16[1,128,2048]{2,1,0:T(8,128)(2,1)S(1)}, bf16[1,128,2048]{2,1,0:T(8,128)(2,1)}, u32[]{:S(2)}) copy-start(bf16[1,128,2048]{2,1,0:T(8,128)(2,1)} %param.36) | copy-start | bytes 1572868
  94.7 30.2 %copy-start.3 = (bf16[1,2048,128]{2,1,0:T(8,128)(2,1)S(1)}, bf16[1,2048,128]{2,1,0:T(8,128)(2,1)}, u32[]{:S(2)}) copy-start(bf16[1,2048,128]{2,1,0:T(8,128)(2,1)} %param.35) | copy-start | bytes 1572868
  159.2 13.6 %copy-start.16 = (f32[128,4]{0,1:T(4,128)S(1)}, f32[128,4]{0,1:T(4,128)}, u32[]{:S(2)}) copy-start(f32[128,4]{0,1:T(4,128)} %param.33) | copy-start | bytes 6148
  159.2 13.8 %copy-start.18 = (s32[128]{0:T(128)S(1)}, s32[128]{0:T(128)}, u32[]{:S(2)}) copy-start(s32[128]{0:T(128)} %copy-done.17) | copy-start | bytes 1540
  160.9 29.6 %all-to-all-start.4 = ((bf16[64,2,2048]{2,1,0:T(2,128)(2,1)}), bf16[64,2,2048]{2,1,0:T(2,128)(2,1)S(1)}, u32[]{:S(2)}, u32[]{:S(2)}) async-start(bf16[64,2,2048]{2,1,0:T(2,128)(2,1)} %copy.153), calls=%async_computation.4 | async-start | bytes 1048576 | tf_op jit(solution)/shard_map/all_to_all | solution.py:202
  194.5 3.5 %copy-start.13 = (f32[2048]{0:T(1024)S(1)}, f32[2048]{0:T(1024)}, u32[]{:S(2)}) copy-start(f32[2048]{0:T(1024)} %param.41) | copy-start | bytes 24580
  194.5 3.5 %copy-start.14 = (f32[2048]{0:T(1024)S(1)}, f32[2048]{0:T(1024)}, u32[]{:S(2)}) copy-start(f32[2048]{0:T(1024)} %param.40) | copy-start | bytes 24580
Sparse Core Ops, SparseCore 0:
  94.9 27.6 all-gather.2
where the time goes:
time: 207 us; the launch traced here: 206 us
  waiting for transfers between devices  58.8 us (28%)
  blocking collectives  52.1 us (25%)
  starting transfers between devices  32 us (15%)
  local copies, waits for them, and re-layouts  19.8 us (10%)
  matrix products  15.4 us (7%)
  between operations  14.3 us (7%)
  other arithmetic  13.3 us (6%)
    all_to_all x1, blocking collectives, summed_on_arrival(): lax.all_to_all(cut_along(shard, dim, count), axis, 0, 0, tiled=True)  28.9 us
    all_gather x1, waiting for transfers between devices, shards(): fanned = lax.all_gather(arrived[None], 'tp', axis=0, tiled=True)  27.8 us
    all_to_all x1, blocking collectives, shards(): lax.all_to_all(outgoing, 'sp', split_axis=0, concat_axis=0, tiled=True)  23.1 us
    all_to_all x1, waiting for transfers between devices, shards(): lax.all_to_all(leaving, 'sp', split_axis=0, concat_axis=0, tiled=True)  14.8 us
    all_to_all x1, starting transfers between devices, shards(): lax.all_to_all(leaving, 'sp', split_axis=0, concat_axis=0, tiled=True)  11.9 us
    all_to_all x1, starting transfers between devices, copy_for_each(): lax.all_to_all(jnp.broadcast_to(shard[None], (count, *shard.shape)), axis...  11.3 us
    all_to_all x1, waiting for transfers between devices, summed_on_arrival(): lax.all_to_all(cut_along(shard, dim, count), axis, 0, 0, tiled=True)  8.83 us
    all_to_all x1, waiting for transfers between devices, copy_for_each(): lax.all_to_all(jnp.broadcast_to(shard[None], (count, *shard.shape)), axis...  7.34 us
  transfers between devices with their start and end apart: 5, of which 4 were waited for; matrix products, arithmetic and copies ran while one was open for 6% of the time, Pallas kernels for 0%

commit v1 on v0

--- a/solution.py
+++ b/solution.py
@@ -5,6 +5,11 @@
 
 RESIDUAL_SCALE = 8.0**0.25
 NORM_EPSILON = 1e-05
+
+
+def gather_by_exchange(array, axis, dim):
+    copies = jnp.concatenate([array] * lax.axis_size(axis), axis=dim)
+    return lax.all_to_all(copies, axis, dim, dim, tiled=True)
 
 
 def copy_for_each(shard, axis):
@@ -192,7 +197,7 @@
     outgoing = jnp.take(padded_rows, table, axis=0).reshape(expert_count, capacity, width)
     arrived = lax.all_to_all(outgoing, "sp", split_axis=0, concat_axis=0, tiled=True)
     slots = arrived.shape[1]
-    fanned = lax.all_gather(arrived[None], "tp", axis=0, tiled=True)
+    fanned = gather_by_exchange(arrived[None], "tp", 0)
     shaped = fanned.reshape(tp_count, -1, local_count, slots, width)
     partial_value = expert_terms(
         shaped, "xslc", routed_gate_weight, routed_up_weight, routed_down_weight

time: 207 us -> 188 us (0.908)
  blocking collectives: 52.1 us -> 80.5 us
  waiting for transfers between devices: 58.8 us -> 31.1 us
  between operations: 14.3 us -> 0.87 us
  starting transfers between devices: 32 us -> 27.2 us
    all_to_all x0 -> x1, blocking collectives: none -> 28.6 us  [gather_by_exchange(): return lax.all_to_all(copies, axis, dim, dim, tiled=True)]
    all_gather x1 -> x0, waiting for transfers between devices: 27.8 us -> none  [shards(): fanned = lax.all_gather(arrived[None], 'tp', axis=0, tiled=True)]
    all_to_all x1, starting transfers between devices: 11.9 us -> 7.11 us  [shards(): lax.all_to_all(leaving, 'sp', split_axis=0, concat_axis=0, tiled=True)]
  transfers between devices with their start and end apart: 5 -> 4, of which waited for: 4 -> 3; matrix products, arithmetic and copies ran while one was open for 6% -> 6% of each run, Pallas kernels for 0% -> 0%
where the time goes in v1:
time: 188 us; the launch traced here: 187 us
  blocking collectives  80.5 us (43%)
  waiting for transfers between devices  31.1 us (17%)
  starting transfers between devices  27.2 us (14%)
  local copies, waits for them, and re-layouts  20.5 us (11%)
  matrix products  14 us (7%)
  other arithmetic  13.3 us (7%)
    all_to_all x1, blocking collectives, summed_on_arrival(): lax.all_to_all(cut_along(shard, dim, count), axis, 0, 0, tiled=True)  28.8 us
    all_to_all x1, blocking collectives, gather_by_exchange(): return lax.all_to_all(copies, axis, dim, dim, tiled=True)  28.6 us
    all_to_all x1, blocking collectives, shards(): lax.all_to_all(outgoing, 'sp', split_axis=0, concat_axis=0, tiled=True)  23.1 us
    all_to_all x1, waiting for transfers between devices, shards(): lax.all_to_all(leaving, 'sp', split_axis=0, concat_axis=0, tiled=True)  14.8 us
    all_to_all x1, starting transfers between devices, copy_for_each(): lax.all_to_all(jnp.broadcast_to(shard[None], (count, *shard.shape)), axis...  11.3 us
    all_to_all x1, waiting for transfers between devices, summed_on_arrival(): lax.all_to_all(cut_along(shard, dim, count), axis, 0, 0, tiled=True)  8.84 us
    all_to_all x1, waiting for transfers between devices, copy_for_each(): lax.all_to_all(jnp.broadcast_to(shard[None], (count, *shard.shape)), axis...  7.4 us
    all_to_all x1, starting transfers between devices, shards(): lax.all_to_all(leaving, 'sp', split_axis=0, concat_axis=0, tiled=True)  7.11 us
  transfers between devices with their start and end apart: 4, of which 3 were waited for; matrix products, arithmetic and copies ran while one was open for 6% of the time, Pallas kernels for 0%

profile of v1, /device:TPU:1, one launch (start us, length us, event | category | flops | bytes accessed | tf_op | source)
XLA Modules:
  0.0 187.5 jit_solution(10463653834387888441)
XLA Ops:
  0.0 1.1 copy.122
  1.1 4.5 %collective-permute-start = (bf16[3,2,256]{2,0,1:T(4,128)(2,1)S(1)}, bf16[3,2,256]{2,0,1:T(4,128)(2,1)S(1)}, u32[]{:S(2)}, u32[]{:S(2)}) collective-permute-start(bf16[3,2,256]{2,0,1:T(4,128)(2,1)S(1)} %slice.395), channel_id=1, source_target_pairs={{0,4},{4,8},{8,12},{12,16},{16,20},{20,24},{24,28},{28,32},{32,36}... | collective-permute-start | bytes 9224 | tf_op jit(solution)/shard_map/ppermute | solution.py:64
  5.6 0.7 convert_element_type.67
  6.3 0.7 fusion.66
  7.0 0.8 copy.139
  7.8 0.7 reshape.138
  8.9 0.3 fusion.11
  9.4 0.3 fusion.7
  9.8 1.0 fusion.83
  11.0 0.6 slice_bitcast_fusion
  11.6 0.6 fusion.81
  12.3 0.8 copy.156
  13.1 1.2 fusion.34
  14.4 0.7 broadcast_in_dim.59
  15.1 11.3 %all-to-all-start = ((f32[64,4,256]{2,1,0:T(4,128)}), f32[64,4,256]{2,1,0:T(4,128)S(1)}, u32[]{:S(2)}, u32[]{:S(2)}) async-start(f32[64,4,256]{2,1,0:T(4,128)} %broadcast_in_dim.59), calls=%async_computation | async-start | bytes 524288 | tf_op jit(solution)/shard_map/all_to_all | solution.py:17
  26.4 0.8 fusion.42
  27.5 0.9 select_reduce_fusion
  28.4 0.7 fusion.72
  29.1 1.4 scatter_custom_fusion
  30.6 0.7 slice.345
  31.3 0.7 slice.343
  32.1 7.4 %all-to-all-done = f32[64,4,256]{2,1,0:T(4,128)S(1)} async-done(((f32[64,4,256]{2,1,0:T(4,128)}), f32[64,4,256]{2,1,0:T(4,128)S(1)}, u32[]{:S(2)}, u32[]{:S(2)}) %all-to-all-start) | async-done | bytes 262176 | tf_op jit(solution)/shard_map/all_to_all | solution.py:17
  39.7 0.6 slice.315
  40.4 0.7 slice.316
  41.1 0.9 fusion.91
  42.5 1.0 fusion.88
  45.2 1.3 fusion.1
  46.5 4.3 %all-to-all-start.1 = ((bf16[4,32,2048]{2,1,0:T(8,128)(2,1)}), bf16[4,32,2048]{2,1,0:T(8,128)(2,1)S(1)}, u32[]{:S(2)}, u32[]{:S(2)}) async-start(bf16[4,32,2048]{2,1,0:T(8,128)(2,1)} %bitcast.17), calls=%async_computation.1 | async-start | bytes 1048576 | tf_op jit(solution)/shard_map/all_to_all | solution.py:75
  51.0 8.8 %all-to-all-done.1 = bf16[4,32,2048]{2,1,0:T(8,128)(2,1)S(1)} async-done(((bf16[4,32,2048]{2,1,0:T(8,128)(2,1)}), bf16[4,32,2048]{2,1,0:T(8,128)(2,1)S(1)}, u32[]{:S(2)}, u32[]{:S(2)}) %all-to-all-start.1) | async-done | bytes 524320 | tf_op jit(solution)/shard_map/all_to_all | solution.py:75
  60.5 0.9 gather_fusion
  61.4 1.1 gather.10
  62.6 1.6 broadcast_select_fusion
  64.2 23.1 %all_to_all.30 = bf16[64,2,2048]{2,1,0:T(2,128)(2,1)S(1)} all-to-all(bf16[64,2,2048]{2,1,0:T(2,128)(2,1)S(1)} %broadcast_select_fusion), channel_id=1, replica_groups=mesh['sp'=64,'tp'=4] {'sp'}, dimensions={0} | all-to-all | bytes 1048576 | tf_op jit(solution)/shard_map/all_to_all | solution.py:198
  87.7 28.6 %all_to_all.31 = bf16[4,64,2,2048]{3,1,2,0:T(8,128)(2,1)S(1)} all-to-all(bf16[4,64,2,2048]{3,1,2,0:T(8,128)(2,1)S(1)} %concatenate.43), channel_id=1, replica_groups=mesh['sp'=64,'tp'=4] {'tp'}, dimensions={0} | all-to-all | bytes 4194304 | tf_op jit(solution)/shard_map/all_to_all | solution.py:12
  116.4 1.3 copy-done.1
  117.7 0.7 convolution_bitcast_fusion.2
  118.4 5.5 %fusion = bf16[4,1,64,1,2,2048]{5,2,4,3,1,0:T(8,128)(2,1)} fusion(bf16[4,64,2,2048]{3,1,2,0:T(8,128)(2,1)} %copy-done.1, bf16[1,128,2048]{2,1,0:T(8,128)(2,1)} %param.36, bf16[1,2048,128]{2,1,0:T(8,128)(2,1)} %param.35, f32[4,64,1,2,128]{4,1,3,0,2:T(8,128)S(1)} %convolution_bitcast_fusion.2), kind=kOutput, calls=%fused_computation.4 | convolution fusion | flops 538312704 | bytes 5505024 | tf_op jit(solution)/shard_map/xslcf,lfd->xslcd/dot_general | solution.py:109
  123.9 28.8 %all_to_all.32 = bf16[4,1,64,1,2,2048]{5,2,4,3,1,0:T(8,128)(2,1)S(1)} all-to-all(bf16[4,1,64,1,2,2048]{5,2,4,3,1,0:T(8,128)(2,1)} %fusion), channel_id=1, replica_groups=mesh['sp'=64,'tp'=4] {'tp'}, dimensions={0} | all-to-all | bytes 4194304 | tf_op jit(solution)/shard_map/all_to_all | solution.py:75
  152.6 0.4 bitcast_reduce_fusion
  153.0 1.3 copy.143
  154.3 7.1 %all-to-all-start.5 = ((bf16[64,2,2048]{2,1,0:T(2,128)(2,1)}), bf16[64,2,2048]{2,1,0:T(2,128)(2,1)S(1)}, u32[]{:S(2)}, u32[]{:S(2)}) async-start(bf16[64,2,2048]{2,1,0:T(2,128)(2,1)} %copy.143), calls=%async_computation.5 | async-start | bytes 1048576 | tf_op jit(solution)/shard_map/all_to_all | solution.py:207
  161.6 2.7 %fusion.100 = f32[32,512]{1,0:T(8,128)} fusion(bf16[32,2048]{1,0:T(8,128)(2,1)S(1)} %add_convert_fusion.1, bf16[2048,512]{1,0:T(8,128)(2,1)} %param.37), kind=kOutput, calls=%fused_computation.188 | convolution fusion | flops 67108864 | bytes 2293760 | tf_op jit(solution)/shard_map/dot_general | solution.py:216
  164.3 14.8 %all-to-all-done.5 = bf16[64,2,2048]{2,1,0:T(2,128)(2,1)S(1)} async-done(((bf16[64,2,2048]{2,1,0:T(2,128)(2,1)}), bf16[64,2,2048]{2,1,0:T(2,128)(2,1)S(1)}, u32[]{:S(2)}, u32[]{:S(2)}) %all-to-all-start.5) | async-done | bytes 524320 | tf_op jit(solution)/shard_map/all_to_all | solution.py:207
  179.3 1.7 gather_fusion.1
  181.1 1.4 reshape.145
  182.4 0.7 multiply_reduce_fusion
  183.2 3.3 %fusion.99 = (f32[32]{0:T(128)S(1)}, f32[32,2048]{1,0:T(8,128)S(1)}) fusion(f32[32,2048]{1,0:T(8,128)S(1)} %multiply_reduce_fusion, bf16[512,2048]{1,0:T(8,128)(2,1)} %param.39, bf16[32,2048]{1,0:T(8,128)(2,1)S(1)} %add_convert_fusion.1, bf16[2048,512]{1,0:T(8,128)(2,1)} %param.38, f32[32,512]{1,0:T(8,128)} %fusion.100), kind=kOutput, calls=%fused_computation.187 | convolution fusion | flops 134643680 | bytes 4915328 | tf_op jit(solution)/shard_map/dot_general | solution.py:219
  186.7 0.8 add_convert_fusion
  (180 shorter events, 5.3 us)
Async XLA Ops:
  0.0 45.2 %copy-start = (bf16[2,256,2048]{2,1,0:T(8,128)(2,1)S(1)}, bf16[2,256,2048]{2,1,0:T(8,128)(2,1)}, u32[]{:S(2)}) copy-start(bf16[2,256,2048]{2,1,0:T(8,128)(2,1)} %param.29) | copy-start | bytes 6291460
  0.0 8.9 %copy-start.19 = (bf16[2,4,64,64]{3,2,1,0:T(8,128)(2,1)S(1)}, bf16[2,4,64,64]{3,2,1,0:T(8,128)(2,1)}, u32[]{:S(2)}) copy-start(bf16[2,4,64,64]{3,2,1,0:T(8,128)(2,1)} %param.25) | copy-start | bytes 196612
  1.1 7.4 %collective-permute-start = (bf16[3,2,256]{2,0,1:T(4,128)(2,1)S(1)}, bf16[3,2,256]{2,0,1:T(4,128)(2,1)S(1)}, u32[]{:S(2)}, u32[]{:S(2)}) collective-permute-start(bf16[3,2,256]{2,0,1:T(4,128)(2,1)S(1)} %slice.395), channel_id=1, source_target_pairs={{0,4},{4,8},{8,12},{12,16},{16,20},{20,24},{24,28},{28,32},{32,36}... | collective-permute-start | bytes 9224 | tf_op jit(solution)/shard_map/ppermute | solution.py:64
  6.3 2.5 %copy-start.7 = (f32[2,256]{1,0:T(2,128)}, f32[2,256]{1,0:T(2,128)S(1)}, u32[]{:S(2)}) copy-start(f32[2,256]{1,0:T(2,128)S(1)} %get-tuple-element.37) | copy-start | bytes 6148
  6.3 2.5 %copy-start.8 = (f32[2,256]{1,0:T(2,128)}, f32[2,256]{1,0:T(2,128)S(1)}, u32[]{:S(2)}) copy-start(f32[2,256]{1,0:T(2,128)S(1)} %get-tuple-element.38) | copy-start | bytes 6148
  6.3 2.5 %copy-start.9 = (f32[2,256]{1,0:T(2,128)}, f32[2,256]{1,0:T(2,128)S(1)}, u32[]{:S(2)}) copy-start(f32[2,256]{1,0:T(2,128)S(1)} %get-tuple-element.39) | copy-start | bytes 6148
  6.3 2.5 %copy-start.10 = (f32[2,256]{1,0:T(2,128)}, f32[2,256]{1,0:T(2,128)S(1)}, u32[]{:S(2)}) copy-start(f32[2,256]{1,0:T(2,128)S(1)} %get-tuple-element.40) | copy-start | bytes 6148
  8.5 0.9 copy-start.20
  13.1 1.2 copy-start.15
  15.1 24.4 %all-to-all-start = ((f32[64,4,256]{2,1,0:T(4,128)}), f32[64,4,256]{2,1,0:T(4,128)S(1)}, u32[]{:S(2)}, u32[]{:S(2)}) async-start(f32[64,4,256]{2,1,0:T(4,128)} %broadcast_in_dim.59), calls=%async_computation | async-start | bytes 524288 | tf_op jit(solution)/shard_map/all_to_all | solution.py:17
  29.1 13.0 %copy-start.17 = (s32[128]{0:T(128)}, s32[128]{0:T(128)S(1)}, u32[]{:S(2)}) copy-start(s32[128]{0:T(128)S(1)} %fusion.72) | copy-start | bytes 1540
  42.4 1.2 copy-start.5
  43.8 1.2 copy-start.6
  44.3 0.9 copy-start.4
  45.2 5.6 %copy-start.21 = (s32[128]{0:T(128)S(1)}, s32[128]{0:T(128)}, u32[]{:S(2)}) copy-start(s32[128]{0:T(128)} %scatter_custom_fusion) | copy-start | bytes 1540
  45.2 14.7 %copy-start.2 = (bf16[32,2048]{1,0:T(8,128)(2,1)S(1)}, bf16[32,2048]{1,0:T(8,128)(2,1)}, u32[]{:S(2)}) copy-start(bf16[32,2048]{1,0:T(8,128)(2,1)} %param.21) | copy-start | bytes 393220
  46.5 13.8 %copy-start.11 = (f32[2048]{0:T(1024)S(1)}, f32[2048]{0:T(1024)}, u32[]{:S(2)}) copy-start(f32[2048]{0:T(1024)} %param.31) | copy-start | bytes 24580
  46.5 13.8 %copy-start.12 = (f32[2048]{0:T(1024)S(1)}, f32[2048]{0:T(1024)}, u32[]{:S(2)}) copy-start(f32[2048]{0:T(1024)} %param.30) | copy-start | bytes 24580
  46.5 13.3 %all-to-all-start.1 = ((bf16[4,32,2048]{2,1,0:T(8,128)(2,1)}), bf16[4,32,2048]{2,1,0:T(8,128)(2,1)S(1)}, u32[]{:S(2)}, u32[]{:S(2)}) async-start(bf16[4,32,2048]{2,1,0:T(8,128)(2,1)} %bitcast.17), calls=%async_computation.1 | async-start | bytes 1048576 | tf_op jit(solution)/shard_map/all_to_all | solution.py:75
  87.7 30.0 %copy-start.3 = (bf16[1,2048,128]{2,1,0:T(8,128)(2,1)S(1)}, bf16[1,2048,128]{2,1,0:T(8,128)(2,1)}, u32[]{:S(2)}) copy-start(bf16[1,2048,128]{2,1,0:T(8,128)(2,1)} %param.34) | copy-start | bytes 1572868
  116.3 1.3 copy-start.1
  152.6 8.8 %copy-start.16 = (f32[128,4]{0,1:T(4,128)S(1)}, f32[128,4]{0,1:T(4,128)}, u32[]{:S(2)}) copy-start(f32[128,4]{0,1:T(4,128)} %param.33) | copy-start | bytes 6148
  152.6 9.0 %copy-start.18 = (s32[128]{0:T(128)S(1)}, s32[128]{0:T(128)}, u32[]{:S(2)}) copy-start(s32[128]{0:T(128)} %copy-done.17) | copy-start | bytes 1540
  154.3 24.8 %all-to-all-start.5 = ((bf16[64,2,2048]{2,1,0:T(2,128)(2,1)}), bf16[64,2,2048]{2,1,0:T(2,128)(2,1)S(1)}, u32[]{:S(2)}, u32[]{:S(2)}) async-start(bf16[64,2,2048]{2,1,0:T(2,128)(2,1)} %copy.143), calls=%async_computation.5 | async-start | bytes 1048576 | tf_op jit(solution)/shard_map/all_to_all | solution.py:207
  183.2 3.5 %copy-start.13 = (f32[2048]{0:T(1024)S(1)}, f32[2048]{0:T(1024)}, u32[]{:S(2)}) copy-start(f32[2048]{0:T(1024)} %param.41) | copy-start | bytes 24580
  183.2 3.5 %copy-start.14 = (f32[2048]{0:T(1024)S(1)}, f32[2048]{0:T(1024)}, u32[]{:S(2)}) copy-start(f32[2048]{0:T(1024)} %param.40) | copy-start | bytes 24580
